TPU v7x, 32 devices: a whole 2x2x4 slice. The times are simulated.
32 devices in a mesh: fs: 16 (over z, y, x), tp: 2 (over core).
Axes of the slice: x: 2, y: 2, z: 4, core: 2. Of those that a mesh axis runs over, the one named last changes fastest.
Arguments:
- tokens: bfloat16 [6144, 2048], P('fs', 'tp'), may hold values from -24 to 24
- mixer_gain: float32 [2048], replicated, may hold values from 0.1 to 1.9
- pool_input: bfloat16 [2048, 1024], P('fs', 'tp'), may hold values from -0.125 to 0.125
- group_weight: bfloat16 [8, 128, 128], P('tp'), may hold values from -0.5 to 0.5
- channel_scale: float32 [1024], P('tp'), may hold values from 0.5 to 2
- pool_output: bfloat16 [1024, 2048], P('tp', 'fs'), may hold values from -0.1875 to 0.1875
- ffn_gain: float32 [2048], replicated, may hold values from 0.1 to 1.9
- gate_weight: bfloat16 [2048, 5632], P('fs', 'tp'), may hold values from -0.125 to 0.125
- up_weight: bfloat16 [2048, 5632], P('fs', 'tp'), may hold values from -0.125 to 0.125
- down_weight: bfloat16 [5632, 2048], P('tp', 'fs'), may hold values from -0.078125 to 0.078125
- final_gain: float32 [2048], P('tp'), may hold values from 0.1 to 1.9
Outputs:
- normed_out: bfloat16 [6144, 2048], P('fs', 'tp')
All inputs are finite; a program needn't handle non-finite values.
Results may differ from a plain program's by a relative error of at most 0.015.
Values may be sent and summed in bfloat16 or wider, within the bound.
No kernel may reach another device: no remote copies, remote signals or barrier semaphores. Data moves between devices by JAX's collectives and lax.ppermute only.
A program may use at most 128 MiB of HBM per device.

v0:
```python
import jax
import jax.numpy as jnp
from jax import lax
from jax.sharding import PartitionSpec as P

D = 2048
GROUP_DIM = 128
LENGTH = 128
EPS = 1e-06


def rms(values, gain):
    wide = values.astype(jnp.float32)
    scaled = wide * lax.rsqrt(jnp.mean(wide * wide, axis=-1, keepdims=True) + EPS)
    return scaled * gain


def add_rows(left, piece):
    return jnp.dot(left, piece, preferred_element_type=jnp.float32)


def local(
    tokens,
    mixer_gain,
    pool_input,
    group_weight,
    channel_scale,
    pool_output,
    ffn_gain,
    gate_weight,
    up_weight,
    down_weight,
    final_gain,
):
    full_rows = lax.all_gather(tokens, "tp", axis=1, tiled=True)
    first_normed = rms(full_rows, mixer_gain).astype(jnp.bfloat16)
    row_count = first_normed.shape[0]
    pooled_in = add_rows(first_normed, lax.all_gather(pool_input, "fs", axis=0, tiled=True)).astype(
        jnp.bfloat16
    )
    local_groups = group_weight.shape[0]
    group_ids = lax.axis_index("tp") * local_groups + jnp.arange(local_groups, dtype=jnp.int32)
    windows = jnp.left_shift(jnp.int32(2), group_ids % 4)
    later = jnp.arange(LENGTH, dtype=jnp.int32)[None, :, None]
    earlier = jnp.arange(LENGTH, dtype=jnp.int32)[None, None, :]
    reach = windows[:, None, None]
    inside = (earlier <= later) & (earlier > later - reach)
    band = inside.astype(jnp.bfloat16)
    divisor = jnp.minimum(later[:, :, 0] + 1, windows[:, None]).astype(jnp.float32)
    grid_low = pooled_in.reshape(row_count // LENGTH, LENGTH, local_groups, GROUP_DIM)
    window_sums = jnp.einsum("gts,nsgc->ntgc", band, grid_low, preferred_element_type=jnp.float32)
    average = window_sums / jnp.transpose(divisor)[None, :, :, None]
    pooled = (
        (average - grid_low.astype(jnp.float32))
        .astype(jnp.bfloat16)
        .reshape(row_count, local_groups, GROUP_DIM)
    )
    mapped = jnp.einsum("ngc,gcd->ngd", pooled, group_weight, preferred_element_type=jnp.float32)
    grouped = (mapped.reshape(row_count, local_groups * GROUP_DIM) * channel_scale).astype(
        jnp.bfloat16
    )
    mixer_terms = jnp.dot(
        grouped,
        lax.all_gather(pool_output, "fs", axis=1, tiled=True),
        preferred_element_type=jnp.float32,
    )
    mixer_out = lax.psum_scatter(
        mixer_terms.astype(jnp.bfloat16), "tp", scatter_dimension=1, tiled=True
    ).astype(jnp.float32)
    middle = (tokens.astype(jnp.float32) + mixer_out).astype(jnp.bfloat16)
    middle_rows = lax.all_gather(middle, "tp", axis=1, tiled=True)
    second_normed = rms(middle_rows, ffn_gain).astype(jnp.bfloat16)
    gate = add_rows(second_normed, lax.all_gather(gate_weight, "fs", axis=0, tiled=True))
    upward = add_rows(second_normed, lax.all_gather(up_weight, "fs", axis=0, tiled=True))
    hidden = (jax.nn.silu(gate) * upward).astype(jnp.bfloat16)
    ffn_terms = jnp.dot(
        hidden,
        lax.all_gather(down_weight, "fs", axis=1, tiled=True),
        preferred_element_type=jnp.float32,
    )
    ffn_out = lax.psum_scatter(
        ffn_terms.astype(jnp.bfloat16), "tp", scatter_dimension=1, tiled=True
    ).astype(jnp.float32)
    closing = middle.astype(jnp.float32) + ffn_out
    squares = lax.psum(jnp.sum(closing * closing, axis=1, keepdims=True), "tp")
    scaled = closing * lax.rsqrt(squares / D + EPS) * final_gain
    return scaled.astype(jnp.bfloat16)


def solution(mesh):
    placed = (
        P("fs", "tp"),
        P(),
        P("fs", "tp"),
        P("tp", None, None),
        P("tp"),
        P("tp", "fs"),
        P(),
        P("fs", "tp"),
        P("fs", "tp"),
        P("tp", "fs"),
        P("tp"),
    )
    return jax.shard_map(
        local, mesh=mesh, in_specs=placed, out_specs=P("fs", "tp"), check_vma=False
    )
```

profile of v0, /device:TPU:0, one launch (start us, length us, event | category | flops | bytes accessed | tf_op | source)
XLA Modules:
  0.0 684.9 jit_solution(15526173825975011963)
XLA Ops:
  6.5 0.7 all-gather.8.cloned.1.call-update
  7.3 0.7 all-gather.10.cloned.1.call-update
  8.1 0.7 all-gather.12.cloned.1.call-update
  8.8 0.1 iota_subtract_fusion
  8.9 0.1 minimum_convert_fusion
  9.0 12.4 %all-gather.8.cloned.1.call-done = bf16[384,2048]{1,0:T(8,128)(2,1)} async-done(((bf16[384,1024]{1,0:T(8,128)(2,1)}), bf16[384,2048]{1,0:T(8,128)(2,1)}) %all-gather.8.cloned.1.call-update) | async-done | bytes 1572880 | tf_op jit(solution)/shard_map/all_gather | solution.py:35
  21.4 1.8 fusion.1
  23.2 62.6 %all-gather.10.cloned.1.call-done = bf16[2048,512]{1,0:T(8,128)(2,1)} async-done(((bf16[128,512]{1,0:T(8,128)(2,1)}), bf16[2048,512]{1,0:T(8,128)(2,1)}) %all-gather.10.cloned.1.call-update) | async-done | bytes 2097168 | tf_op jit(solution)/shard_map/all_gather | solution.py:38
  85.8 3.1 fusion.14
  88.9 0.1 reshape.132
  89.0 0.3 fusion.13
  89.3 0.3 fusion.31
  89.7 0.1 fusion.17
  89.8 60.4 %all-gather.12.cloned.1.call-done = bf16[512,2048]{1,0:T(8,128)(2,1)} async-done(((bf16[512,128]{1,0:T(8,128)(2,1)}), bf16[512,2048]{1,0:T(8,128)(2,1)}) %all-gather.12.cloned.1.call-update) | async-done | bytes 2097168 | tf_op jit(solution)/shard_map/all_gather | solution.py:64
  150.3 3.8 convolution_convert_fusion.1
  154.1 7.2 %reduce-scatter.3.cloned.1.call-done = bf16[384,1024]{1,0:T(8,128)(2,1)} async-done(((bf16[384,2048]{1,0:T(8,128)(2,1)}), bf16[384,1024]{1,0:T(8,128)(2,1)}) %reduce-scatter.3.cloned.1.call-update) | async-done | bytes 786448 | tf_op jit(solution)/shard_map/reduce_scatter | solution.py:67
  161.4 2.3 add_convert_fusion
  163.7 0.5 all-gather.16.cloned.1.call-update
  164.3 0.7 all-gather.18.cloned.1.call-update
  165.1 0.7 all-gather.20.cloned.1.call-update
  165.8 0.2 reduce-scatter.5.cloned.1.call-start
  166.0 8.9 %all-gather.14.cloned.1.call-done = bf16[384,2048]{1,0:T(8,128)(2,1)} async-done(((bf16[384,1024]{1,0:T(8,128)(2,1)}), bf16[384,2048]{1,0:T(8,128)(2,1)}) %all-gather.14.cloned.1.call-update) | async-done | bytes 1572880 | tf_op jit(solution)/shard_map/all_gather | solution.py:71
  174.9 1.8 fusion.4
  176.7 143.4 %all-gather.16.cloned.1.call-done = bf16[2048,2816]{1,0:T(8,128)(2,1)} async-done(((bf16[128,2816]{1,0:T(8,128)(2,1)}), bf16[2048,2816]{1,0:T(8,128)(2,1)}) %all-gather.16.cloned.1.call-update) | async-done | bytes 11534352 | tf_op jit(solution)/shard_map/all_gather | solution.py:73
  320.2 11.5 %fusion.20 = f32[384,2816]{1,0:T(8,128)} fusion(bf16[2048,2816]{1,0:T(8,128)(2,1)} %all-gather.16.cloned.1.call-done, bf16[384,2048]{1,0:T(8,128)(2,1)} %all-gather.14.cloned.1.call-done, f32[2048]{0:T(1024)S(1)} %copy-done.6, f32[384]{0:T(512)S(1)} %add_rsqrt_fusion), kind=kOutput, calls=%fused_computation.28 | convolution fusion | flops 4432330752 | bytes 17442304 | tf_op jit(solution)/shard_map/dot_general | solution.py:19
  331.7 130.8 %all-gather.18.cloned.1.call-done = bf16[2048,2816]{1,0:T(8,128)(2,1)} async-done(((bf16[128,2816]{1,0:T(8,128)(2,1)}), bf16[2048,2816]{1,0:T(8,128)(2,1)}) %all-gather.18.cloned.1.call-update) | async-done | bytes 11534352 | tf_op jit(solution)/shard_map/all_gather | solution.py:74
  462.5 183.0 %all-gather.20.cloned.1.call-done = bf16[2816,2048]{1,0:T(8,128)(2,1)} async-done(((bf16[2816,128]{1,0:T(8,128)(2,1)}), bf16[2816,2048]{1,0:T(8,128)(2,1)}) %all-gather.20.cloned.1.call-update) | async-done | bytes 11534352 | tf_op jit(solution)/shard_map/all_gather | solution.py:78
  645.5 19.3 %convolution_convert_fusion = bf16[384,2048]{1,0:T(8,128)(2,1)} fusion(bf16[2816,2048]{1,0:T(8,128)(2,1)} %all-gather.20.cloned.1.call-done, bf16[2048,2816]{1,0:T(8,128)(2,1)} %all-gather.18.cloned.1.call-done, f32[384,2816]{1,0:T(8,128)} %fusion.20, bf16[384,2048]{1,0:T(8,128)(2,1)S(1)} %copy-done.3, f32[2048]{0:T(1024)S(1)} %copy-done.6, ...), kind=kOutput, calls=%fused_computation.12 | convolution fusion | flops 8868790272 | bytes 30549504 | tf_op jit(solution)/shard_map/dot_general | solution.py:76
  664.8 7.3 %reduce-scatter.5.cloned.1.call-done = bf16[384,1024]{1,0:T(8,128)(2,1)} async-done(((bf16[384,2048]{1,0:T(8,128)(2,1)}), bf16[384,1024]{1,0:T(8,128)(2,1)}) %reduce-scatter.5.cloned.1.call-update) | async-done | bytes 786448 | tf_op jit(solution)/shard_map/reduce_scatter | solution.py:81
  672.1 1.5 multiply_reduce_fusion
  673.6 2.5 psum.7
  676.1 2.3 multiply_convert_fusion
  (32 shorter events, 0.4 us)
Async XLA Ops:
  6.5 82.8 %copy-start = (bf16[4,128,128]{2,1,0:T(8,128)(2,1)S(1)}, bf16[4,128,128]{2,1,0:T(8,128)(2,1)}, u32[]{:S(2)}) copy-start(bf16[4,128,128]{2,1,0:T(8,128)(2,1)} %param.14) | copy-start | bytes 393220
  6.5 14.9 %all-gather.8.cloned.1.call-start = ((), (), s32[]{:S(2)}) async-start(), calls=%async_computation.2 | async-start | bytes 2359296 | tf_op jit(solution)/shard_map/all_gather | solution.py:35
  7.3 78.5 %all-gather.10.cloned.1.call-start = ((), (), s32[]{:S(2)}) async-start(), calls=%async_computation.3 | async-start | bytes 2228224 | tf_op jit(solution)/shard_map/all_gather | solution.py:38
  8.0 142.3 %all-gather.12.cloned.1.call-start = ((), (), s32[]{:S(2)}) async-start(), calls=%async_computation.4 | async-start | bytes 2228224 | tf_op jit(solution)/shard_map/all_gather | solution.py:64
  8.7 152.6 %reduce-scatter.3.cloned.1.call-start = ((), (), s32[]{:S(2)}) async-start(), calls=%async_computation.5 | async-start | bytes 2359296 | tf_op jit(solution)/shard_map/reduce_scatter | solution.py:67
  88.9 0.8 copy-start.5
  89.7 71.7 %copy-start.2 = (bf16[384,1024]{1,0:T(8,128)(2,1)S(1)}, bf16[384,1024]{1,0:T(8,128)(2,1)}, u32[]{:S(2)}) copy-start(bf16[384,1024]{1,0:T(8,128)(2,1)} %param.11) | copy-start | bytes 2359300
  154.1 166.1 %copy-start.6 = (f32[2048]{0:T(1024)S(1)}, f32[2048]{0:T(1024)}, u32[]{:S(2)}) copy-start(f32[2048]{0:T(1024)} %param.17) | copy-start | bytes 24580
  154.1 20.8 %all-gather.14.cloned.1.call-start = ((), (), s32[]{:S(2)}) async-start(), calls=%async_computation.6 | async-start | bytes 2359296 | tf_op jit(solution)/shard_map/all_gather | solution.py:71
  163.7 156.5 %all-gather.16.cloned.1.call-start = ((), (), s32[]{:S(2)}) async-start(), calls=%async_computation.7 | async-start | bytes 12255232 | tf_op jit(solution)/shard_map/all_gather | solution.py:73
  164.3 298.3 %all-gather.18.cloned.1.call-start = ((), (), s32[]{:S(2)}) async-start(), calls=%async_computation.8 | async-start | bytes 12255232 | tf_op jit(solution)/shard_map/all_gather | solution.py:74
  165.0 480.5 %all-gather.20.cloned.1.call-start = ((), (), s32[]{:S(2)}) async-start(), calls=%async_computation.9 | async-start | bytes 12255232 | tf_op jit(solution)/shard_map/all_gather | solution.py:78
  165.8 506.3 %reduce-scatter.5.cloned.1.call-start = ((), (), s32[]{:S(2)}) async-start(), calls=%async_computation.10 | async-start | bytes 2359296 | tf_op jit(solution)/shard_map/reduce_scatter | solution.py:81
  176.7 468.8 %copy-start.3 = (bf16[384,2048]{1,0:T(8,128)(2,1)S(1)}, bf16[384,2048]{1,0:T(8,128)(2,1)}, u32[]{:S(2)}) copy-start(bf16[384,2048]{1,0:T(8,128)(2,1)} %all-gather.14.cloned.1.call-done) | copy-start | bytes 4718596
  331.7 340.4 %copy-start.1 = (bf16[384,1024]{1,0:T(8,128)(2,1)S(1)}, bf16[384,1024]{1,0:T(8,128)(2,1)}, u32[]{:S(2)}) copy-start(bf16[384,1024]{1,0:T(8,128)(2,1)} %add_convert_fusion) | copy-start | bytes 2359300
  664.8 11.3 %copy-start.4 = (f32[1024]{0:T(1024)S(1)}, f32[1024]{0:T(1024)}, u32[]{:S(2)}) copy-start(f32[1024]{0:T(1024)} %param.21) | copy-start | bytes 12292
Sparse Core Ops, SparseCore 0:
  8.9 12.5 all-gather.7
  24.2 61.5 all-gather.9
  88.5 61.7 all-gather.11
  154.2 7.1 reduce-scatter.2
  163.8 11.0 all-gather.13
  177.5 142.5 all-gather.15
  322.9 139.5 all-gather.17
  465.3 180.2 all-gather.19
  664.9 7.1 reduce-scatter.4
where the time goes:
time: 685 us
  waiting for transfers between devices  620 us (91%)
  matrix products  38.3 us (6%)
  between operations  13.3 us (2%)
  other arithmetic  10 us (1%)
    all_gather x1, waiting for transfers between devices, local(): lax.all_gather(down_weight, 'fs', axis=1, tiled=True)  183 us
    all_gather x1, waiting for transfers between devices, local(): lax.all_gather(gate_weight, 'fs', axis=0, tiled=True)  143 us
    all_gather x1, waiting for transfers between devices, local(): lax.all_gather(up_weight, 'fs', axis=0, tiled=True)  131 us
    all_gather x1, waiting for transfers between devices, local(): lax.all_gather(pool_input, 'fs', axis=0, tiled=True)  62.6 us
    all_gather x1, waiting for transfers between devices, local(): lax.all_gather(pool_output, 'fs', axis=1, tiled=True)  60.4 us
    dot_general x1, matrix products, local(): jnp.dot(hidden, lax.all_gather(down_weight, 'fs', axis=1, tiled=True), pr...  19.3 us
    dot_general x2, matrix products, add_rows(): return jnp.dot(left, piece, preferred_element_type=jnp.float32)  14.6 us
  transfers between devices with their start and end apart: 9, of which 9 were waited for; matrix products, arithmetic and copies ran while one was open for 3% of the time, Pallas kernels for 0%

commit v1 on v0

--- a/solution.py
+++ b/solution.py
@@ -75,7 +75,7 @@
     hidden = (jax.nn.silu(gate) * upward).astype(jnp.bfloat16)
     ffn_terms = jnp.dot(
         hidden,
-        lax.all_gather(down_weight, "fs", axis=1, tiled=True),
+        jnp.concatenate(lax.all_gather(down_weight, "fs"), axis=1),
         preferred_element_type=jnp.float32,
     )
     ffn_out = lax.psum_scatter(

time: 685 us -> 647 us (0.945)
  waiting for transfers between devices: 620 us -> 566 us
  local copies, waits for them, and re-layouts: 0.13 us -> 15.5 us
    all_gather x1, waiting for transfers between devices: 183 us -> 143 us  [local(): lax.all_gather(down_weight, 'fs')]
    all_gather x1, waiting for transfers between devices: 143 us -> 127 us  [local(): lax.all_gather(gate_weight, 'fs', axis=0, tiled=True)]
    reshape x0 -> x1, local copies, waits for them, and re-layouts: none -> 15.3 us  [local(): jnp.concatenate(lax.all_gather(down_weight, 'fs'), axis=1)]
  transfers between devices with their start and end apart: 9 -> 9, of which waited for: 9 -> 9; matrix products, arithmetic and copies ran while one was open for 3% -> 5% of each run, Pallas kernels for 0% -> 0%
where the time goes in v1:
time: 647 us
  waiting for transfers between devices  566 us (87%)
  matrix products  38.7 us (6%)
  local copies, waits for them, and re-layouts  15.5 us (2%)
  between operations  13.3 us (2%)
  other arithmetic  10 us (2%)
    all_gather x1, waiting for transfers between devices, local(): lax.all_gather(down_weight, 'fs')  143 us
    all_gather x1, waiting for transfers between devices, local(): lax.all_gather(up_weight, 'fs', axis=0, tiled=True)  133 us
    all_gather x1, waiting for transfers between devices, local(): lax.all_gather(gate_weight, 'fs', axis=0, tiled=True)  127 us
    all_gather x1, waiting for transfers between devices, local(): lax.all_gather(pool_input, 'fs', axis=0, tiled=True)  62.6 us
    all_gather x1, waiting for transfers between devices, local(): lax.all_gather(pool_output, 'fs', axis=1, tiled=True)  60.4 us
    dot_general x1, matrix products, local(): jnp.dot(hidden, jnp.concatenate(lax.all_gather(down_weight, 'fs'), axis=1...  21.5 us
    reshape x1, local copies, waits for them, and re-layouts, local(): jnp.concatenate(lax.all_gather(down_weight, 'fs'), axis=1)  15.3 us
  transfers between devices with their start and end apart: 9, of which 9 were waited for; matrix products, arithmetic and copies ran while one was open for 5% of the time, Pallas kernels for 0%

profile of v1, /device:TPU:0, one launch (start us, length us, event | category | flops | bytes accessed | tf_op | source)
XLA Modules:
  0.0 646.6 jit_solution(9722449035734698221)
XLA Ops:
  6.5 0.7 all-gather.9.cloned.1.call-update
  7.3 0.7 all-gather.11.cloned.1.call-update
  8.1 0.7 all-gather.13.cloned.1.call-update
  8.8 0.1 iota_subtract_fusion
  8.9 0.1 minimum_convert_fusion
  9.0 12.4 %all-gather.9.cloned.1.call-done = bf16[384,2048]{1,0:T(8,128)(2,1)} async-done(((bf16[384,1024]{1,0:T(8,128)(2,1)}), bf16[384,2048]{1,0:T(8,128)(2,1)}) %all-gather.9.cloned.1.call-update) | async-done | bytes 1572880 | tf_op jit(solution)/shard_map/all_gather | solution.py:35
  21.4 1.8 fusion.1
  23.2 62.6 %all-gather.11.cloned.1.call-done = bf16[2048,512]{1,0:T(8,128)(2,1)} async-done(((bf16[128,512]{1,0:T(8,128)(2,1)}), bf16[2048,512]{1,0:T(8,128)(2,1)}) %all-gather.11.cloned.1.call-update) | async-done | bytes 2097168 | tf_op jit(solution)/shard_map/all_gather | solution.py:38
  85.8 3.1 fusion.14
  88.9 0.1 reshape.138
  89.0 0.3 fusion.13
  89.3 0.3 fusion.31
  89.7 0.1 fusion.17
  89.8 60.4 %all-gather.13.cloned.1.call-done = bf16[512,2048]{1,0:T(8,128)(2,1)} async-done(((bf16[512,128]{1,0:T(8,128)(2,1)}), bf16[512,2048]{1,0:T(8,128)(2,1)}) %all-gather.13.cloned.1.call-update) | async-done | bytes 2097168 | tf_op jit(solution)/shard_map/all_gather | solution.py:64
  150.3 3.8 convolution_convert_fusion.1
  154.1 7.2 %reduce-scatter.3.cloned.1.call-done = bf16[384,1024]{1,0:T(8,128)(2,1)} async-done(((bf16[384,2048]{1,0:T(8,128)(2,1)}), bf16[384,1024]{1,0:T(8,128)(2,1)}) %reduce-scatter.3.cloned.1.call-update) | async-done | bytes 786448 | tf_op jit(solution)/shard_map/reduce_scatter | solution.py:67
  161.3 2.3 add_convert_fusion
  163.7 0.5 all-gather.21.cloned.1.call-update
  164.3 0.7 all-gather.17.cloned.1.call-update
  165.1 0.7 all-gather.19.cloned.1.call-update
  165.8 9.1 %all-gather.15.cloned.1.call-done = bf16[384,2048]{1,0:T(8,128)(2,1)} async-done(((bf16[384,1024]{1,0:T(8,128)(2,1)}), bf16[384,2048]{1,0:T(8,128)(2,1)}) %all-gather.15.cloned.1.call-update) | async-done | bytes 1572880 | tf_op jit(solution)/shard_map/all_gather | solution.py:71
  174.9 1.8 fusion.4
  176.7 143.4 %all-gather.21.cloned.1.call-done = bf16[45056,128]{1,0:T(8,128)(2,1)} async-done(((bf16[2816,128]{1,0:T(8,128)(2,1)}), bf16[45056,128]{1,0:T(8,128)(2,1)}) %all-gather.21.cloned.1.call-update) | async-done | bytes 11534352 | tf_op jit(solution)/shard_map/all_gather | solution.py:78
  320.2 15.3 %copy.21 = bf16[2816,16,128]{0,2,1:T(8,128)(2,1)} copy(bf16[2816,16,128]{2,0,1:T(8,128)(2,1)} %bitcast.32) | data formatting | bytes 23068672 | tf_op jit(solution)/shard_map/reshape | solution.py:78
  335.5 127.0 %all-gather.17.cloned.1.call-done = bf16[2048,2816]{1,0:T(8,128)(2,1)} async-done(((bf16[128,2816]{1,0:T(8,128)(2,1)}), bf16[2048,2816]{1,0:T(8,128)(2,1)}) %all-gather.17.cloned.1.call-update) | async-done | bytes 11534352 | tf_op jit(solution)/shard_map/all_gather | solution.py:73
  462.5 9.7 %fusion.20 = f32[384,2816]{1,0:T(8,128)} fusion(bf16[2048,2816]{1,0:T(8,128)(2,1)} %all-gather.17.cloned.1.call-done, bf16[384,2048]{1,0:T(8,128)(2,1)S(1)} %copy-done.4, f32[2048]{0:T(1024)S(1)} %copy-done.7, f32[384]{0:T(512)S(1)} %add_rsqrt_fusion), kind=kOutput, calls=%fused_computation.28 | convolution fusion | flops 4432330752 | bytes 17442304 | tf_op jit(solution)/shard_map/dot_general | solution.py:19
  472.2 132.7 %all-gather.19.cloned.1.call-done = bf16[2048,2816]{1,0:T(8,128)(2,1)} async-done(((bf16[128,2816]{1,0:T(8,128)(2,1)}), bf16[2048,2816]{1,0:T(8,128)(2,1)}) %all-gather.19.cloned.1.call-update) | async-done | bytes 11534352 | tf_op jit(solution)/shard_map/all_gather | solution.py:74
  604.9 21.5 %convolution_convert_fusion = bf16[384,2048]{1,0:T(8,128)(2,1)} fusion(bf16[2816,2048]{0,1:T(8,128)(2,1)} %bitcast.33, bf16[2048,2816]{1,0:T(8,128)(2,1)} %all-gather.19.cloned.1.call-done, f32[384,2816]{1,0:T(8,128)} %fusion.20, bf16[384,2048]{1,0:T(8,128)(2,1)S(1)} %copy-done.4, f32[2048]{0:T(1024)S(1)} %copy-done.7, f32[384]{0:T(512)S(1)} %add_rsqrt_fusion), kind=kOutput, calls=%fused_computation.12 | convolution fusion | flops 8868790272 | bytes 30549504 | tf_op jit(solution)/shard_map/dot_general | solution.py:76
  626.5 7.3 %reduce-scatter.5.cloned.1.call-done = bf16[384,1024]{1,0:T(8,128)(2,1)} async-done(((bf16[384,2048]{1,0:T(8,128)(2,1)}), bf16[384,1024]{1,0:T(8,128)(2,1)}) %reduce-scatter.5.cloned.1.call-update) | async-done | bytes 786448 | tf_op jit(solution)/shard_map/reduce_scatter | solution.py:81
  633.8 1.5 multiply_reduce_fusion
  635.2 2.5 psum.7
  637.7 2.3 multiply_convert_fusion
  (35 shorter events, 0.5 us)
Async XLA Ops:
  6.5 82.8 %copy-start = (bf16[4,128,128]{2,1,0:T(8,128)(2,1)S(1)}, bf16[4,128,128]{2,1,0:T(8,128)(2,1)}, u32[]{:S(2)}) copy-start(bf16[4,128,128]{2,1,0:T(8,128)(2,1)} %param.14) | copy-start | bytes 393220
  6.5 14.9 %all-gather.9.cloned.1.call-start = ((), (), s32[]{:S(2)}) async-start(), calls=%async_computation.2 | async-start | bytes 2359296 | tf_op jit(solution)/shard_map/all_gather | solution.py:35
  7.3 78.5 %all-gather.11.cloned.1.call-start = ((), (), s32[]{:S(2)}) async-start(), calls=%async_computation.3 | async-start | bytes 2228224 | tf_op jit(solution)/shard_map/all_gather | solution.py:38
  8.0 142.3 %all-gather.13.cloned.1.call-start = ((), (), s32[]{:S(2)}) async-start(), calls=%async_computation.4 | async-start | bytes 2228224 | tf_op jit(solution)/shard_map/all_gather | solution.py:64
  8.7 152.6 %reduce-scatter.3.cloned.1.call-start = ((), (), s32[]{:S(2)}) async-start(), calls=%async_computation.5 | async-start | bytes 2359296 | tf_op jit(solution)/shard_map/reduce_scatter | solution.py:67
  88.9 0.8 copy-start.6
  89.7 71.7 %copy-start.3 = (bf16[384,1024]{1,0:T(8,128)(2,1)S(1)}, bf16[384,1024]{1,0:T(8,128)(2,1)}, u32[]{:S(2)}) copy-start(bf16[384,1024]{1,0:T(8,128)(2,1)} %param.11) | copy-start | bytes 2359300
  154.1 20.9 %all-gather.15.cloned.1.call-start = ((), (), s32[]{:S(2)}) async-start(), calls=%async_computation.6 | async-start | bytes 2359296 | tf_op jit(solution)/shard_map/all_gather | solution.py:71
  163.7 156.5 %all-gather.21.cloned.1.call-start = ((), (), s32[]{:S(2)}) async-start(), calls=%async_computation.10 | async-start | bytes 12255232 | tf_op jit(solution)/shard_map/all_gather | solution.py:78
  164.3 298.3 %all-gather.17.cloned.1.call-start = ((), (), s32[]{:S(2)}) async-start(), calls=%async_computation.7 | async-start | bytes 12255232 | tf_op jit(solution)/shard_map/all_gather | solution.py:73
  165.0 439.9 %all-gather.19.cloned.1.call-start = ((), (), s32[]{:S(2)}) async-start(), calls=%async_computation.8 | async-start | bytes 12255232 | tf_op jit(solution)/shard_map/all_gather | solution.py:74
  165.8 468.0 %reduce-scatter.5.cloned.1.call-start = ((), (), s32[]{:S(2)}) async-start(), calls=%async_computation.9 | async-start | bytes 2359296 | tf_op jit(solution)/shard_map/reduce_scatter | solution.py:81
  320.2 142.4 %copy-start.4 = (bf16[384,2048]{1,0:T(8,128)(2,1)S(1)}, bf16[384,2048]{1,0:T(8,128)(2,1)}, u32[]{:S(2)}) copy-start(bf16[384,2048]{1,0:T(8,128)(2,1)} %all-gather.15.cloned.1.call-done) | copy-start | bytes 4718596
  320.2 142.4 %copy-start.7 = (f32[2048]{0:T(1024)S(1)}, f32[2048]{0:T(1024)}, u32[]{:S(2)}) copy-start(f32[2048]{0:T(1024)} %param.17) | copy-start | bytes 24580
  604.9 28.8 %copy-start.2 = (bf16[384,1024]{1,0:T(8,128)(2,1)S(1)}, bf16[384,1024]{1,0:T(8,128)(2,1)}, u32[]{:S(2)}) copy-start(bf16[384,1024]{1,0:T(8,128)(2,1)} %add_convert_fusion) | copy-start | bytes 2359300
  604.9 35.1 %copy-start.1 = (bf16[4,128,128]{2,1,0:T(8,128)(2,1)S(1)}, bf16[4,128,128]{2,1,0:T(8,128)(2,1)}, u32[]{:S(2)}) copy-start(bf16[4,128,128]{2,1,0:T(8,128)(2,1)} %param.14) | copy-start | bytes 393220
  626.4 11.3 %copy-start.5 = (f32[1024]{0:T(1024)S(1)}, f32[1024]{0:T(1024)}, u32[]{:S(2)}) copy-start(f32[1024]{0:T(1024)} %param.21) | copy-start | bytes 12292
Sparse Core Ops, SparseCore 0:
  8.9 12.5 all-gather.8
  24.2 61.5 all-gather.10
  88.5 61.7 all-gather.12
  154.2 7.1 reduce-scatter.2
  163.8 11.0 all-gather.14
  177.5 142.5 all-gather.20
  322.9 139.5 all-gather.16
  465.3 139.5 all-gather.18
  626.6 7.1 reduce-scatter.4
